TPU v7x, 32 devices: a whole 2x2x4 slice. The times are simulated.
32 devices in a mesh: sp: 8 (over z, y), tp: 4 (over x, core).
Axes of the slice: x: 2, y: 2, z: 4, core: 2. Of those that a mesh axis runs over, the one named last changes fastest.
Arguments:
- hidden_states: bfloat16 [4096, 4096], P('sp', 'tp'), may hold values from -6 to 6
- pre_gain: float32 [2, 4096], replicated, may hold values from 0.1 to 1.9
- post_gain: float32 [2, 4096], P(None, 'tp'), may hold values from 0.1 to 1.9
- w_value: bfloat16 [2, 4096, 2048], P(None, 'sp', 'tp'), may hold values from -0.09375 to 0.09375
- w_outer: bfloat16 [2, 4096, 2048], P(None, 'sp', 'tp'), may hold values from -0.09375 to 0.09375
- w_inner: bfloat16 [2, 4096, 2048], P(None, 'sp', 'tp'), may hold values from -0.09375 to 0.09375
- taps: float32 [2, 3, 2048], P(None, None, 'tp'), may hold values from -3 to 3
- w_out: bfloat16 [2, 2048, 4096], P(None, 'tp', 'sp'), as said below
Outputs:
- final_states: bfloat16 [4096, 4096], P('sp', 'tp')
Inputs may be any that keep to these rules, and one draw needn't show every extreme that they name: `w_out`: independent entries; the columns fall into 8 groups of 512 consecutive columns, each group with its own scale.
All inputs are finite; a program needn't handle non-finite values.
Results may differ from a plain program's by a relative error of at most 0.024.
Values may be sent and summed in bfloat16 or wider, within the bound.
A program may use at most 128 MiB of HBM per device.

v0:
```python
import jax
import jax.numpy as jnp
from jax import lax
from jax.sharding import PartitionSpec as P

D = 4096
eps = 1e-06


def passed_along(value, axis, by):
    size = lax.axis_size(axis)
    pairs = [(i, i + by) for i in range(size) if 0 <= i + by < size]
    return lax.ppermute(value, axis, pairs)


def local(hidden_states, pre_gain, post_gain, w_value, w_outer, w_inner, taps, w_out):
    current = hidden_states
    layers = w_value.shape[0]
    whole_value, whole_outer, whole_inner, whole_out = (
        lax.all_gather(w_value, "sp", axis=1, tiled=True),
        lax.all_gather(w_outer, "sp", axis=1, tiled=True),
        lax.all_gather(w_inner, "sp", axis=1, tiled=True),
        lax.all_gather(w_out, "sp", axis=2, tiled=True),
    )
    for layer_index in range(layers):
        gathered = lax.all_gather(current, "tp", axis=1, tiled=True)
        widened = gathered.astype(jnp.float32)
        normed = (
            widened
            * lax.rsqrt(jnp.mean(widened * widened, axis=1, keepdims=True) + eps)
            * pre_gain[layer_index]
        ).astype(jnp.bfloat16)
        value_proj = jnp.dot(normed, whole_value[layer_index], preferred_element_type=jnp.float32)
        outer_proj = jnp.dot(normed, whole_outer[layer_index], preferred_element_type=jnp.float32)
        inner_proj = jnp.dot(normed, whole_inner[layer_index], preferred_element_type=jnp.float32)
        gated_input = (inner_proj * value_proj).astype(jnp.bfloat16)
        before = passed_along(gated_input[-2:], "sp", 1)
        extended = jnp.concatenate([before, gated_input], axis=0).astype(jnp.float32)
        length = gated_input.shape[0]
        kernel = taps[layer_index]
        convolved = (
            extended[0:length] * kernel[0]
            + extended[1 : length + 1] * kernel[1]
            + extended[2 : length + 2] * kernel[2]
        )
        conv_out = (outer_proj * convolved).astype(jnp.bfloat16)
        partial_terms = jnp.dot(
            conv_out, whole_out[layer_index], preferred_element_type=jnp.float32
        )
        mixed = lax.psum_scatter(
            partial_terms.astype(jnp.bfloat16), "tp", scatter_dimension=1, tiled=True
        ).astype(jnp.float32)
        power = lax.psum(jnp.sum(mixed * mixed, axis=1), "tp")
        rescale = lax.rsqrt(power / D + eps)
        current = (
            current.astype(jnp.float32) + mixed * rescale[:, None] * post_gain[layer_index]
        ).astype(jnp.bfloat16)
    return current


def solution(mesh):
    placed = (
        P("sp", "tp"),
        P(),
        P(None, "tp"),
        P(None, "sp", "tp"),
        P(None, "sp", "tp"),
        P(None, "sp", "tp"),
        P(None, None, "tp"),
        P(None, "tp", "sp"),
    )
    return jax.shard_map(
        local, mesh=mesh, in_specs=placed, out_specs=P("sp", "tp"), check_vma=False
    )
```

profile of v0, /device:TPU:0, one launch (start us, length us, event | category | flops | bytes accessed | tf_op | source)
XLA Modules:
  0.0 729.6 jit_solution(7224380522898905791)
XLA Ops:
  6.5 0.7 all-gather.7.cloned.1.call-update
  7.3 0.0 all-gather.13.cloned.1.call-start
  7.3 0.7 all-gather.13.cloned.1.call-update
  8.0 0.0 all-gather.11.cloned.1.call-start
  8.1 0.7 all-gather.11.cloned.1.call-update
  8.7 0.0 all-gather.9.cloned.1.call-start
  8.8 0.5 all-gather.9.cloned.1.call-update
  9.3 0.0 all-gather.15.cloned.1.call-start
  9.4 0.5 all-gather.15.cloned.1.call-update
  9.9 0.0 reduce-scatter.3.cloned.1.call-start
  10.0 36.1 %all-gather.7.cloned.1.call-done = bf16[512,4096]{1,0:T(8,128)(2,1)} async-done(((bf16[512,1024]{1,0:T(8,128)(2,1)}), bf16[512,4096]{1,0:T(8,128)(2,1)}) %all-gather.7.cloned.1.call-update) | async-done | bytes 4194320 | tf_op jit(solution)/shard_map/all_gather | solution.py:26
  46.1 3.1 fusion
  49.2 123.6 %all-gather.13.cloned.1.call-done = bf16[2,4096,512]{2,1,0:T(8,128)(2,1)} async-done(((bf16[2,512,512]{2,1,0:T(8,128)(2,1)}), bf16[2,4096,512]{2,1,0:T(8,128)(2,1)}) %all-gather.13.cloned.1.call-update) | async-done | bytes 8388624 | tf_op jit(solution)/shard_map/all_gather | solution.py:20
  172.8 5.8 fusion.9
  178.6 119.0 %all-gather.11.cloned.1.call-done = bf16[2,4096,512]{2,1,0:T(8,128)(2,1)} async-done(((bf16[2,512,512]{2,1,0:T(8,128)(2,1)}), bf16[2,4096,512]{2,1,0:T(8,128)(2,1)}) %all-gather.11.cloned.1.call-update) | async-done | bytes 8388624 | tf_op jit(solution)/shard_map/all_gather | solution.py:22
  297.6 5.8 fusion.26
  303.5 2.5 collective-permute-start
  306.0 1.3 collective-permute-done
  307.3 0.2 maximum_convert_fusion
  307.4 114.9 %all-gather.9.cloned.1.call-done = bf16[2,4096,512]{2,1,0:T(8,128)(2,1)} async-done(((bf16[2,512,512]{2,1,0:T(8,128)(2,1)}), bf16[2,4096,512]{2,1,0:T(8,128)(2,1)}) %all-gather.9.cloned.1.call-update) | async-done | bytes 8388624 | tf_op jit(solution)/shard_map/all_gather | solution.py:21
  422.4 6.0 fusion.27
  428.4 119.0 %all-gather.15.cloned.1.call-done = bf16[2,512,4096]{2,1,0:T(8,128)(2,1)} async-done(((bf16[2,512,512]{2,1,0:T(8,128)(2,1)}), bf16[2,512,4096]{2,1,0:T(8,128)(2,1)}) %all-gather.15.cloned.1.call-update) | async-done | bytes 8388624 | tf_op jit(solution)/shard_map/all_gather | solution.py:23
  547.4 6.7 convolution_convert_fusion.1
  554.1 0.0 reduce-scatter.3.cloned.1.call-update
  554.1 0.0 all-gather.17.cloned.1.call-start
  554.1 0.6 copy-done.5
  554.8 42.1 %reduce-scatter.3.cloned.1.call-done = bf16[512,1024]{1,0:T(8,128)(2,1)} async-done(((bf16[512,4096]{1,0:T(8,128)(2,1)}), bf16[512,1024]{1,0:T(8,128)(2,1)}) %reduce-scatter.3.cloned.1.call-update) | async-done | bytes 1048592 | tf_op jit(solution)/shard_map/reduce_scatter | solution.py:50
  596.8 1.5 fusion.12
  598.3 5.8 psum.14
  604.1 2.6 fusion.15
  606.7 0.0 all-gather.17.cloned.1.call-update
  606.8 0.2 reduce-scatter.5.cloned.1.call-start
  607.0 35.0 %all-gather.17.cloned.1.call-done = bf16[512,4096]{1,0:T(8,128)(2,1)} async-done(((bf16[512,1024]{1,0:T(8,128)(2,1)}), bf16[512,4096]{1,0:T(8,128)(2,1)}) %all-gather.17.cloned.1.call-update) | async-done | bytes 4194320 | tf_op jit(solution)/shard_map/all_gather | solution.py:26
  642.0 3.2 fusion.3
  645.2 0.2 copy-done.1
  645.4 4.7 fusion.6
  650.2 4.7 fusion.24
  655.0 3.4 collective-permute-start.1
  658.3 1.3 collective-permute-done.1
  659.6 0.2 maximum_convert_fusion.1
  659.8 2.6 fusion.25
  662.4 0.7 slice-done.1
  663.2 4.3 convolution_convert_fusion
  667.5 0.0 reduce-scatter.5.cloned.1.call-update
  667.5 45.4 %reduce-scatter.5.cloned.1.call-done = bf16[512,1024]{1,0:T(8,128)(2,1)} async-done(((bf16[512,4096]{1,0:T(8,128)(2,1)}), bf16[512,1024]{1,0:T(8,128)(2,1)}) %reduce-scatter.5.cloned.1.call-update) | async-done | bytes 1048592 | tf_op jit(solution)/shard_map/reduce_scatter | solution.py:50
  712.9 1.5 fusion.16
  714.4 5.8 psum.15
  720.1 2.6 fusion.19
  (29 shorter events, 0.1 us)
Async XLA Ops:
  6.5 3.4 copy-start.3
  6.5 39.6 %all-gather.7.cloned.1.call-start = ((), (), s32[]{:S(2)}) async-start(), calls=%async_computation.2 | async-start | bytes 5242880 | tf_op jit(solution)/shard_map/all_gather | solution.py:26
  7.3 165.5 %all-gather.13.cloned.1.call-start = ((), (), s32[]{:S(2)}) async-start(), calls=%async_computation.5 | async-start | bytes 9437184 | tf_op jit(solution)/shard_map/all_gather | solution.py:20
  8.0 289.6 %all-gather.11.cloned.1.call-start = ((), (), s32[]{:S(2)}) async-start(), calls=%async_computation.4 | async-start | bytes 9437184 | tf_op jit(solution)/shard_map/all_gather | solution.py:22
  8.7 413.6 %all-gather.9.cloned.1.call-start = ((), (), s32[]{:S(2)}) async-start(), calls=%async_computation.3 | async-start | bytes 9437184 | tf_op jit(solution)/shard_map/all_gather | solution.py:21
  9.3 538.1 %all-gather.15.cloned.1.call-start = ((), (), s32[]{:S(2)}) async-start(), calls=%async_computation.6 | async-start | bytes 9437184 | tf_op jit(solution)/shard_map/all_gather | solution.py:23
  9.9 586.9 %reduce-scatter.3.cloned.1.call-start = ((), (), s32[]{:S(2)}) async-start(), calls=%async_computation.7 | async-start | bytes 5242880 | tf_op jit(solution)/shard_map/reduce_scatter | solution.py:50
  178.6 127.4 %copy-start.4 = (f32[2,3,512]{2,0,1:T(2,128)S(1)}, f32[2,3,512]{2,0,1:T(2,128)}, u32[]{:S(2)}) copy-start(f32[2,3,512]{2,0,1:T(2,128)} %param.14) | copy-start | bytes 36868
  303.5 3.8 collective-permute-start
  554.1 0.7 copy-start.5
  554.1 50.0 %copy-start.2 = (bf16[512,1024]{1,0:T(8,128)(2,1)S(1)}, bf16[512,1024]{1,0:T(8,128)(2,1)}, u32[]{:S(2)}) copy-start(bf16[512,1024]{1,0:T(8,128)(2,1)} %param.8) | copy-start | bytes 3145732
  554.1 87.9 %all-gather.17.cloned.1.call-start = ((), (), s32[]{:S(2)}) async-start(), calls=%async_computation.8 | async-start | bytes 5242880 | tf_op jit(solution)/shard_map/all_gather | solution.py:26
  606.8 106.1 %reduce-scatter.5.cloned.1.call-start = ((), (), s32[]{:S(2)}) async-start(), calls=%async_computation.9 | async-start | bytes 5242880 | tf_op jit(solution)/shard_map/reduce_scatter | solution.py:50
  642.0 3.4 copy-start.1
  645.4 14.4 %slice-start.2 = ((s8[8388608]{0:T(1024)(128)(4,1)}), s8[4194304]{0:T(1024)(128)(4,1)S(1)}, s32[]{:S(2)}) async-start(s8[8388608]{0:T(1024)(128)(4,1)} %bitcast.68), calls=%async_computation.12 | async-start | bytes 8388608
  650.2 9.6 %slice-start.3 = ((s8[8388608]{0:T(1024)(128)(4,1)}), s8[4194304]{0:T(1024)(128)(4,1)S(1)}, s32[]{:S(2)}) async-start(s8[8388608]{0:T(1024)(128)(4,1)} %bitcast.68), calls=%async_computation.13 | async-start | bytes 8388608
  655.0 4.7 collective-permute-start.1
  659.6 2.8 slice-start
  659.8 3.3 slice-start.1
  667.5 52.7 %copy-start = (bf16[512,1024]{1,0:T(8,128)(2,1)S(1)}, bf16[512,1024]{1,0:T(8,128)(2,1)}, u32[]{:S(2)}) copy-start(bf16[512,1024]{1,0:T(8,128)(2,1)} %fusion.15) | copy-start | bytes 3145732
Sparse Core Ops, SparseCore 0:
  8.9 37.1 all-gather.6
  48.3 124.4 all-gather.12
  175.0 122.6 all-gather.10
  299.7 122.6 all-gather.8
  424.2 123.1 all-gather.14
  554.2 42.5 reduce-scatter.2
  606.9 35.0 all-gather.16
  667.6 45.2 reduce-scatter.4
where the time goes:
time: 730 us
  waiting for transfers between devices  641 us (88%)
  matrix products  40.7 us (6%)
  other arithmetic  14.9 us (2%)
  between operations  13.7 us (2%)
  blocking collectives  11.5 us (2%)
    all_gather x1, waiting for transfers between devices, local(): lax.all_gather(w_value, 'sp', axis=1, tiled=True)  124 us
    all_gather x1, waiting for transfers between devices, local(): lax.all_gather(w_out, 'sp', axis=2, tiled=True)  119 us
    all_gather x1, waiting for transfers between devices, local(): lax.all_gather(w_inner, 'sp', axis=1, tiled=True)  119 us
    all_gather x1, waiting for transfers between devices, local(): lax.all_gather(w_outer, 'sp', axis=1, tiled=True)  115 us
    reduce_scatter x2, waiting for transfers between devices, local(): lax.psum_scatter(partial_terms.astype(jnp.bfloat16), 'tp', scatter_dimens...  87.4 us
    all_gather x2, waiting for transfers between devices, local(): gathered = lax.all_gather(current, 'tp', axis=1, tiled=True)  71.1 us
  transfers between devices with their start and end apart: 10, of which 10 were waited for; matrix products, arithmetic and copies ran while one was open for 3% of the time, Pallas kernels for 0%

commit v1 on v0

--- a/solution.py
+++ b/solution.py
@@ -1,3 +1,4 @@
+import functools
 import jax
 import jax.numpy as jnp
 from jax import lax
@@ -5,6 +6,22 @@
 
 D = 4096
 eps = 1e-06
+
+
+def change_racks_here(xin, link_axis, which_dim):
+    full_n = lax.axis_size(link_axis)
+    main = xin
+    sheets = [main]
+    block_next = sorted(((dev, (dev + 1) % full_n) for dev in range(full_n)))
+    for c in range(1, full_n):
+        main = lax.ppermute(main, link_axis, block_next)
+        sheets.insert(0, main)
+    latest = jnp.concatenate(sheets, which_dim)
+    reached = jnp.roll(latest, (lax.axis_index(link_axis) + 1) * xin.shape[which_dim], which_dim)
+    return reached
+
+
+scan_cards_for = functools.partial(change_racks_here, link_axis="tp", which_dim=1)
 
 
 def passed_along(value, axis, by):
@@ -23,7 +40,7 @@
         lax.all_gather(w_out, "sp", axis=2, tiled=True),
     )
     for layer_index in range(layers):
-        gathered = lax.all_gather(current, "tp", axis=1, tiled=True)
+        gathered = scan_cards_for(current)
         widened = gathered.astype(jnp.float32)
         normed = (
             widened

time: 730 us -> 703 us (0.963)
  waiting for transfers between devices: 641 us -> 607 us
  other arithmetic: 14.9 us -> 23.3 us
    ppermute x0 -> x6, waiting for transfers between devices: none -> 84.8 us  [change_racks_here(): main = lax.ppermute(main, link_axis, block_next)]
    all_gather x2 -> x0, waiting for transfers between devices: 71.1 us -> none  [local(): gathered = lax.all_gather(current, 'tp', axis=1, tiled=True)]
    all_gather x1, waiting for transfers between devices: 124 us -> 75.5 us  [local(): lax.all_gather(w_value, 'sp', axis=1, tiled=True)]
    reduce_sum x2, other arithmetic: 6.31 us -> 15.7 us  [local(): jnp.mean(widened * widened, axis=1, keepdims=True) + eps]
  transfers between devices with their start and end apart: 10 -> 14, of which waited for: 10 -> 14; matrix products, arithmetic and copies ran while one was open for 3% -> 4% of each run, Pallas kernels for 0% -> 0%
where the time goes in v1:
time: 703 us; the launch traced here: 702 us
  waiting for transfers between devices  607 us (86%)
  matrix products  38.2 us (5%)
  other arithmetic  23.3 us (3%)
  between operations  13.7 us (2%)
  blocking collectives  11.5 us (2%)
    all_gather x1, waiting for transfers between devices, local(): lax.all_gather(w_out, 'sp', axis=2, tiled=True)  119 us
    all_gather x1, waiting for transfers between devices, local(): lax.all_gather(w_inner, 'sp', axis=1, tiled=True)  119 us
    all_gather x1, waiting for transfers between devices, local(): lax.all_gather(w_outer, 'sp', axis=1, tiled=True)  115 us
    reduce_scatter x2, waiting for transfers between devices, local(): lax.psum_scatter(partial_terms.astype(jnp.bfloat16), 'tp', scatter_dimens...  88.5 us
    ppermute x6, waiting for transfers between devices, change_racks_here(): main = lax.ppermute(main, link_axis, block_next)  84.8 us
    all_gather x1, waiting for transfers between devices, local(): lax.all_gather(w_value, 'sp', axis=1, tiled=True)  75.5 us
    reduce_sum x2, other arithmetic, local(): jnp.mean(widened * widened, axis=1, keepdims=True) + eps  15.7 us
  transfers between devices with their start and end apart: 14, of which 14 were waited for; matrix products, arithmetic and copies ran while one was open for 4% of the time, Pallas kernels for 0%

profile of v1, /device:TPU:0, one launch (start us, length us, event | category | flops | bytes accessed | tf_op | source)
XLA Modules:
  0.0 702.4 jit_solution(18023685906502437581)
XLA Ops:
  6.5 0.7 all-gather.9.cloned.1.call-update
  7.3 0.0 all-gather.7.cloned.1.call-start
  7.3 0.7 all-gather.7.cloned.1.call-update
  8.0 0.0 all-gather.5.cloned.1.call-start
  8.1 0.7 all-gather.5.cloned.1.call-update
  8.7 0.0 all-gather.11.cloned.1.call-start
  8.8 0.5 all-gather.11.cloned.1.call-update
  9.3 0.0 reduce-scatter.3.cloned.1.call-start
  9.4 0.5 collective-permute-start
  9.9 14.6 %collective-permute-done = bf16[512,1024]{1,0:T(8,128)(2,1)S(1)} collective-permute-done((bf16[512,1024]{1,0:T(8,128)(2,1)}, bf16[512,1024]{1,0:T(8,128)(2,1)S(1)}, u32[]{:S(2)}, u32[]{:S(2)}) %collective-permute-start) | collective-permute-done | bytes 1048608 | tf_op jit(solution)/shard_map/ppermute | solution.py:17
  24.5 0.0 collective-permute-start.1
  24.6 14.2 %collective-permute-done.1 = bf16[512,1024]{1,0:T(8,128)(2,1)S(1)} collective-permute-done((bf16[512,1024]{1,0:T(8,128)(2,1)S(1)}, bf16[512,1024]{1,0:T(8,128)(2,1)S(1)}, u32[]{:S(2)}, u32[]{:S(2)}) %collective-permute-start.1) | collective-permute-done | bytes 1048608 | tf_op jit(solution)/shard_map/ppermute | solution.py:17
  38.7 0.9 fusion.54
  39.6 13.4 %collective-permute-done.2 = bf16[512,1024]{1,0:T(8,128)(2,1)S(1)} collective-permute-done((bf16[512,1024]{1,0:T(8,128)(2,1)S(1)}, bf16[512,1024]{1,0:T(8,128)(2,1)S(1)}, u32[]{:S(2)}, u32[]{:S(2)}) %collective-permute-start.2) | collective-permute-done | bytes 1048608 | tf_op jit(solution)/shard_map/ppermute | solution.py:17
  53.0 8.2 %fusion = (f32[512]{0:T(512)S(1)}, bf16[512,4096]{1,0:T(8,128)(2,1)}) fusion(s32[]{:T(128)S(6)} %select_n.13, bf16[512,1024]{1,0:T(8,128)(2,1)} %param.10, bf16[512,1024]{1,0:T(8,128)(2,1)S(1)} %collective-permute-done, bf16[512,1024]{1,0:T(8,128)(2,1)S(1)} %collective-permute-done.1, bf16[512,1024]{1,0:T(8,128)(2,1)S(1)} %collective-permute-done.2), kind=kLoop, calls=%fused_computation.4 | loop fusion | flops 39845376 | bytes 8390660 | tf_op jit(solution)/shard_map/reduce_sum | solution.py:47
  61.2 75.5 %all-gather.9.cloned.1.call-done = bf16[2,4096,512]{2,1,0:T(8,128)(2,1)} async-done(((bf16[2,512,512]{2,1,0:T(8,128)(2,1)}), bf16[2,4096,512]{2,1,0:T(8,128)(2,1)}) %all-gather.9.cloned.1.call-update) | async-done | bytes 8388624 | tf_op jit(solution)/shard_map/all_gather | solution.py:37
  136.7 5.8 fusion.23
  142.6 119.0 %all-gather.7.cloned.1.call-done = bf16[2,4096,512]{2,1,0:T(8,128)(2,1)} async-done(((bf16[2,512,512]{2,1,0:T(8,128)(2,1)}), bf16[2,4096,512]{2,1,0:T(8,128)(2,1)}) %all-gather.7.cloned.1.call-update) | async-done | bytes 8388624 | tf_op jit(solution)/shard_map/all_gather | solution.py:39
  261.6 5.8 fusion.40
  267.4 2.5 collective-permute-start.3
  269.9 1.3 collective-permute-done.3
  271.2 0.2 maximum_convert_fusion
  271.4 115.1 %all-gather.5.cloned.1.call-done = bf16[2,4096,512]{2,1,0:T(8,128)(2,1)} async-done(((bf16[2,512,512]{2,1,0:T(8,128)(2,1)}), bf16[2,4096,512]{2,1,0:T(8,128)(2,1)}) %all-gather.5.cloned.1.call-update) | async-done | bytes 8388624 | tf_op jit(solution)/shard_map/all_gather | solution.py:38
  386.4 6.0 fusion.41
  392.5 119.0 %all-gather.11.cloned.1.call-done = bf16[2,512,4096]{2,1,0:T(8,128)(2,1)} async-done(((bf16[2,512,512]{2,1,0:T(8,128)(2,1)}), bf16[2,512,4096]{2,1,0:T(8,128)(2,1)}) %all-gather.11.cloned.1.call-update) | async-done | bytes 8388624 | tf_op jit(solution)/shard_map/all_gather | solution.py:40
  511.5 6.6 convolution_convert_fusion.1
  518.1 0.0 reduce-scatter.5.cloned.1.call-start
  518.2 42.7 %reduce-scatter.3.cloned.1.call-done = bf16[512,1024]{1,0:T(8,128)(2,1)} async-done(((bf16[512,4096]{1,0:T(8,128)(2,1)}), bf16[512,1024]{1,0:T(8,128)(2,1)}) %reduce-scatter.3.cloned.1.call-update) | async-done | bytes 1048592 | tf_op jit(solution)/shard_map/reduce_scatter | solution.py:67
  560.9 1.5 fusion.26
  562.4 5.8 psum.14
  568.1 1.7 fusion.29
  569.8 0.1 collective-permute-start.4
  569.9 14.2 %collective-permute-done.4 = bf16[512,1024]{1,0:T(8,128)(2,1)S(1)} collective-permute-done((bf16[512,1024]{1,0:T(8,128)(2,1)S(1)}, bf16[512,1024]{1,0:T(8,128)(2,1)S(1)}, u32[]{:S(2)}, u32[]{:S(2)}) %collective-permute-start.4) | collective-permute-done | bytes 1048608 | tf_op jit(solution)/shard_map/ppermute | solution.py:17
  584.1 14.2 %collective-permute-done.5 = bf16[512,1024]{1,0:T(8,128)(2,1)S(1)} collective-permute-done((bf16[512,1024]{1,0:T(8,128)(2,1)S(1)}, bf16[512,1024]{1,0:T(8,128)(2,1)S(1)}, u32[]{:S(2)}, u32[]{:S(2)}) %collective-permute-start.5) | collective-permute-done | bytes 1048608 | tf_op jit(solution)/shard_map/ppermute | solution.py:17
  598.3 14.2 %collective-permute-done.6 = bf16[512,1024]{1,0:T(8,128)(2,1)S(1)} collective-permute-done((bf16[512,1024]{1,0:T(8,128)(2,1)S(1)}, bf16[512,1024]{1,0:T(8,128)(2,1)S(1)}, u32[]{:S(2)}, u32[]{:S(2)}) %collective-permute-start.6) | collective-permute-done | bytes 1048608 | tf_op jit(solution)/shard_map/ppermute | solution.py:17
  612.5 7.4 %fusion.3 = (f32[512]{0:T(512)S(1)}, bf16[512,4096]{1,0:T(8,128)(2,1)S(1)}) fusion(s32[]{:T(128)S(6)} %select_n.13, bf16[512,1024]{1,0:T(8,128)(2,1)S(1)} %fusion.29, bf16[512,1024]{1,0:T(8,128)(2,1)S(1)} %collective-permute-done.4, bf16[512,1024]{1,0:T(8,128)(2,1)S(1)} %collective-permute-done.5, bf16[512,1024]{1,0:T(8,128)(2,1)S(1)} %collective-permute-done.6), kind=kLoop, calls=%fused_computation.7 | loop fusion | flops 39845376 | bytes 8390660 | tf_op jit(solution)/shard_map/reduce_sum | solution.py:47
  620.0 4.7 fusion.20
  624.8 2.4 fusion.38
  627.1 3.6 collective-permute-start.7
  630.7 1.3 collective-permute-done.7
  632.0 0.2 maximum_convert_fusion.1
  632.2 2.5 fusion.39
  634.8 0.8 slice-done.1
  635.5 4.3 convolution_convert_fusion
  639.9 45.8 %reduce-scatter.5.cloned.1.call-done = bf16[512,1024]{1,0:T(8,128)(2,1)} async-done(((bf16[512,4096]{1,0:T(8,128)(2,1)}), bf16[512,1024]{1,0:T(8,128)(2,1)}) %reduce-scatter.5.cloned.1.call-update) | async-done | bytes 1048592 | tf_op jit(solution)/shard_map/reduce_scatter | solution.py:67
  685.7 1.5 fusion.30
  687.2 5.8 psum.15
  692.9 2.6 fusion.33
  (34 shorter events, 0.2 us)
Async XLA Ops:
  6.5 130.2 %all-gather.9.cloned.1.call-start = ((), (), s32[]{:S(2)}) async-start(), calls=%async_computation.4 | async-start | bytes 9437184 | tf_op jit(solution)/shard_map/all_gather | solution.py:37
  7.3 254.3 %all-gather.7.cloned.1.call-start = ((), (), s32[]{:S(2)}) async-start(), calls=%async_computation.3 | async-start | bytes 9437184 | tf_op jit(solution)/shard_map/all_gather | solution.py:39
  8.0 378.4 %all-gather.5.cloned.1.call-start = ((), (), s32[]{:S(2)}) async-start(), calls=%async_computation.2 | async-start | bytes 9437184 | tf_op jit(solution)/shard_map/all_gather | solution.py:38
  8.7 502.8 %all-gather.11.cloned.1.call-start = ((), (), s32[]{:S(2)}) async-start(), calls=%async_computation.5 | async-start | bytes 9437184 | tf_op jit(solution)/shard_map/all_gather | solution.py:40
  9.3 551.6 %reduce-scatter.3.cloned.1.call-start = ((), (), s32[]{:S(2)}) async-start(), calls=%async_computation.6 | async-start | bytes 5242880 | tf_op jit(solution)/shard_map/reduce_scatter | solution.py:67
  9.4 15.2 %collective-permute-start = (bf16[512,1024]{1,0:T(8,128)(2,1)}, bf16[512,1024]{1,0:T(8,128)(2,1)S(1)}, u32[]{:S(2)}, u32[]{:S(2)}) collective-permute-start(bf16[512,1024]{1,0:T(8,128)(2,1)} %param.10), channel_id=1, source_target_pairs={{0,1},{1,2},{2,3},{3,0},{4,5},{5,6},{6,7},{7,4},{8,9},{9,10},{10,1... | collective-permute-start | bytes 3145736 | tf_op jit(solution)/shard_map/ppermute | solution.py:17
  24.5 14.2 %collective-permute-start.1 = (bf16[512,1024]{1,0:T(8,128)(2,1)S(1)}, bf16[512,1024]{1,0:T(8,128)(2,1)S(1)}, u32[]{:S(2)}, u32[]{:S(2)}) collective-permute-start(bf16[512,1024]{1,0:T(8,128)(2,1)S(1)} %collective-permute-done), channel_id=1, source_target_pairs={{0,1},{1,2},{2,3},{3,0},{4,5},{5,6},{6,7},{7,4},{8,9},{9,10},{10,1... | collective-permute-start | bytes 3145736 | tf_op jit(solution)/shard_map/ppermute | solution.py:17
  38.7 14.2 %collective-permute-start.2 = (bf16[512,1024]{1,0:T(8,128)(2,1)S(1)}, bf16[512,1024]{1,0:T(8,128)(2,1)S(1)}, u32[]{:S(2)}, u32[]{:S(2)}) collective-permute-start(bf16[512,1024]{1,0:T(8,128)(2,1)S(1)} %collective-permute-done.1), channel_id=1, source_target_pairs={{0,1},{1,2},{2,3},{3,0},{4,5},{5,6},{6,7},{7,4},{8,9},{9,10},{10,1... | collective-permute-start | bytes 3145736 | tf_op jit(solution)/shard_map/ppermute | solution.py:17
  142.6 127.3 %copy-start.1 = (f32[2,3,512]{2,0,1:T(2,128)S(1)}, f32[2,3,512]{2,0,1:T(2,128)}, u32[]{:S(2)}) copy-start(f32[2,3,512]{2,0,1:T(2,128)} %param.16) | copy-start | bytes 36868
  267.4 3.8 collective-permute-start.3
  392.5 125.7 %copy-start.2 = (f32[2,1024]{1,0:T(2,128)S(1)}, f32[2,1024]{1,0:T(2,128)}, u32[]{:S(2)}) copy-start(f32[2,1024]{1,0:T(2,128)} %param.12) | copy-start | bytes 24580
  392.5 175.7 %copy-start = (bf16[512,1024]{1,0:T(8,128)(2,1)S(1)}, bf16[512,1024]{1,0:T(8,128)(2,1)}, u32[]{:S(2)}) copy-start(bf16[512,1024]{1,0:T(8,128)(2,1)} %param.10) | copy-start | bytes 3145732
  518.1 167.5 %reduce-scatter.5.cloned.1.call-start = ((), (), s32[]{:S(2)}) async-start(), calls=%async_computation.7 | async-start | bytes 5242880 | tf_op jit(solution)/shard_map/reduce_scatter | solution.py:67
  569.8 14.3 %collective-permute-start.4 = (bf16[512,1024]{1,0:T(8,128)(2,1)S(1)}, bf16[512,1024]{1,0:T(8,128)(2,1)S(1)}, u32[]{:S(2)}, u32[]{:S(2)}) collective-permute-start(bf16[512,1024]{1,0:T(8,128)(2,1)S(1)} %fusion.29), channel_id=1, source_target_pairs={{0,1},{1,2},{2,3},{3,0},{4,5},{5,6},{6,7},{7,4},{8,9},{9,10},{10,1... | collective-permute-start | bytes 3145736 | tf_op jit(solution)/shard_map/ppermute | solution.py:17
  584.1 14.2 %collective-permute-start.5 = (bf16[512,1024]{1,0:T(8,128)(2,1)S(1)}, bf16[512,1024]{1,0:T(8,128)(2,1)S(1)}, u32[]{:S(2)}, u32[]{:S(2)}) collective-permute-start(bf16[512,1024]{1,0:T(8,128)(2,1)S(1)} %collective-permute-done.4), channel_id=1, source_target_pairs={{0,1},{1,2},{2,3},{3,0},{4,5},{5,6},{6,7},{7,4},{8,9},{9,10},{10,1... | collective-permute-start | bytes 3145736 | tf_op jit(solution)/shard_map/ppermute | solution.py:17
  598.3 14.2 %collective-permute-start.6 = (bf16[512,1024]{1,0:T(8,128)(2,1)S(1)}, bf16[512,1024]{1,0:T(8,128)(2,1)S(1)}, u32[]{:S(2)}, u32[]{:S(2)}) collective-permute-start(bf16[512,1024]{1,0:T(8,128)(2,1)S(1)} %collective-permute-done.5), channel_id=1, source_target_pairs={{0,1},{1,2},{2,3},{3,0},{4,5},{5,6},{6,7},{7,4},{8,9},{9,10},{10,1... | collective-permute-start | bytes 3145736 | tf_op jit(solution)/shard_map/ppermute | solution.py:17
  612.5 12.2 %slice-start.4 = ((s8[8388608]{0:T(1024)(128)(4,1)}), s8[4194304]{0:T(1024)(128)(4,1)S(1)}, s32[]{:S(2)}) async-start(s8[8388608]{0:T(1024)(128)(4,1)} %bitcast.70), calls=%async_computation.12 | async-start | bytes 8388608
  620.0 4.7 slice-start.5
  620.0 12.2 %slice-start.2 = ((s8[8388608]{0:T(1024)(128)(4,1)}), s8[4194304]{0:T(1024)(128)(4,1)S(1)}, s32[]{:S(2)}) async-start(s8[8388608]{0:T(1024)(128)(4,1)} %bitcast.68), calls=%async_computation.10 | async-start | bytes 8388608
  624.7 7.5 %slice-start.3 = ((s8[8388608]{0:T(1024)(128)(4,1)}), s8[4194304]{0:T(1024)(128)(4,1)S(1)}, s32[]{:S(2)}) async-start(s8[8388608]{0:T(1024)(128)(4,1)} %bitcast.68), calls=%async_computation.11 | async-start | bytes 8388608
  627.1 4.9 collective-permute-start.7
  632.0 2.7 slice-start
  632.2 3.3 slice-start.1
Sparse Core Ops, SparseCore 0:
  9.5 127.1 all-gather.8
  138.9 122.6 all-gather.6
  263.8 122.6 all-gather.4
  388.3 123.1 all-gather.10
  518.3 42.5 reduce-scatter.2
  640.0 45.6 reduce-scatter.4
